TPU v7x, 32 devices: a whole 2x2x4 slice. The times are simulated.
32 devices in a mesh: kv: 16 (over z, y, x), tp: 2 (over core).
Axes of the slice: x: 2, y: 2, z: 4, core: 2. Of those that a mesh axis runs over, the one named last changes fastest.
Arguments:
- hidden_in: bfloat16 [64, 2048], P('tp', 'kv'), may hold values from -20 to 20
- gain_before: float32 [2048], P('kv'), may hold values from 0.1 to 1.9
- gate_before: bfloat16 [2048, 5632], P('kv', 'tp'), may hold values from -0.125 to 0.125
- lift_before: bfloat16 [2048, 5632], P('kv', 'tp'), may hold values from -0.125 to 0.125
- drop_before: bfloat16 [5632, 2048], P('tp', 'kv'), may hold values from -0.078125 to 0.078125
- mixer_gain: float32 [2048], P('kv'), may hold values from 0.1 to 1.9
- value_proj: bfloat16 [2048, 2048], P('kv', 'tp'), may hold values from -0.125 to 0.125
- gate_proj: bfloat16 [2048, 2048], P('kv', 'tp'), may hold values from -0.125 to 0.125
- key_proj: bfloat16 [2048, 1024], P('kv', 'tp'), may hold values from -0.125 to 0.125
- query_proj: bfloat16 [2048, 1024], P('kv', 'tp'), may hold values from -0.125 to 0.125
- step_proj: bfloat16 [2048, 32], P('kv'), may hold values from -0.125 to 0.125
- value_taps: float32 [4, 2048], P(None, 'tp'), may hold values from -3 to 3
- key_taps: float32 [4, 1024], P(None, 'tp'), may hold values from -3 to 3
- query_taps: float32 [4, 1024], P(None, 'tp'), may hold values from -3 to 3
- value_past: bfloat16 [64, 3, 2048], P('kv', None, 'tp'), may hold values from -6 to 6
- key_past: bfloat16 [64, 3, 1024], P('kv', None, 'tp'), may hold values from -6 to 6
- query_past: bfloat16 [64, 3, 1024], P('kv', None, 'tp'), may hold values from -6 to 6
- decay_rate: float32 [32], P('tp'), may hold values from 0.05 to 1
- block_state: float32 [64, 32, 64, 128], P('kv', 'tp'), may hold values from -24 to 24
- block_keys: bfloat16 [64, 128, 1024], P('kv', None, 'tp'), may hold values from -6 to 6
- block_values: bfloat16 [64, 128, 2048], P('kv', None, 'tp'), may hold values from -6 to 6
- block_steps: float32 [64, 128, 32], P('kv', None, 'tp'), may hold values from 0.2 to 2
- block_decay: float32 [64, 128, 32], P('kv', None, 'tp'), may hold values from -1.25 to 0
- lengths: int32 [64], P('kv'), may hold values from 1 to 128, 2048 in all
- head_gain: float32 [2048], P('tp'), may hold values from 0.1 to 1.9
- out_proj: bfloat16 [2048, 2048], P('tp', 'kv'), may hold values from -0.125 to 0.125
- gain_after: float32 [2048], P('kv'), may hold values from 0.1 to 1.9
- gate_after: bfloat16 [2048, 5632], P('kv', 'tp'), may hold values from -0.125 to 0.125
- lift_after: bfloat16 [2048, 5632], P('kv', 'tp'), may hold values from -0.125 to 0.125
- drop_after: bfloat16 [5632, 2048], P('tp', 'kv'), may hold values from -0.078125 to 0.078125
Outputs:
- hidden_out: bfloat16 [64, 2048], P('tp', 'kv')
Inputs may be any that keep to these rules, and one draw needn't show every extreme that they name: `lengths`: some sequence has all 128 positions filled.
All inputs are finite; a program needn't handle non-finite values. No bound on the sum of `lengths` on one device may be relied on, other than what follows from the above.
Results may differ from a plain program's by a relative error of at most 0.014.
Values may be sent and summed in bfloat16 or wider, within the bound.
A program may use at most 64 MiB of HBM per device.

v0:
```python
import jax
import jax.numpy as jnp
from jax import lax
from jax.sharding import PartitionSpec as P

D = 2048
GROUPS = 8
HEADS = 32
EPSILON = 1e-06


def gather_rows(rows_in, gain_vec):
    whole_rows = lax.all_gather(rows_in, "tp", axis=0, tiled=True)
    values = whole_rows.astype(jnp.float32)
    squares = jnp.sum(values * values, axis=1)
    scaled = (values * gain_vec[None, :]).astype(jnp.bfloat16)
    return (scaled, squares)


def inverse_scale(totals):
    return lax.rsqrt(totals / D + EPSILON)[:, None]


def own_rows(totals, row_count):
    return lax.dynamic_slice_in_dim(totals, lax.axis_index("kv") * row_count, row_count, 0)


def finish(partial_value):
    return lax.psum_scatter(
        partial_value.astype(jnp.float32).astype(jnp.bfloat16),
        "tp",
        scatter_dimension=0,
        tiled=True,
    ).astype(jnp.float32)


def half_mlp(rows_in, gain_vec, gate_weight, lift_weight, drop_weight):
    scaled, squares = gather_rows(rows_in, gain_vec)
    totals = lax.psum(squares, "kv")
    gate_part = jnp.dot(scaled, gate_weight, preferred_element_type=jnp.float32)
    lift_part = jnp.dot(scaled, lift_weight, preferred_element_type=jnp.float32)
    gate_sum, lift_sum = lax.psum((gate_part, lift_part), "kv")
    row_scale = inverse_scale(totals)
    hidden = (jax.nn.silu(gate_sum * row_scale) * (lift_sum * row_scale)).astype(jnp.bfloat16)
    partial_value = jnp.dot(hidden, drop_weight, preferred_element_type=jnp.float32).astype(
        jnp.bfloat16
    )
    return finish(partial_value)


def convolve(past_rows, taps, newest):
    earlier = jnp.sum(past_rows.astype(jnp.float32) * taps[None, :-1, :], axis=1)
    return jax.nn.silu(earlier + taps[-1][None, :] * newest)


def mixer(
    rows_in,
    mixer_gain,
    value_proj,
    gate_proj,
    key_proj,
    query_proj,
    step_proj,
    value_taps,
    key_taps,
    query_taps,
    value_past,
    key_past,
    query_past,
    decay_rate,
    block_state,
    block_keys,
    block_values,
    block_steps,
    block_decay,
    lengths,
    head_gain,
    out_proj,
):
    scaled, squares = gather_rows(rows_in, mixer_gain)
    seq_count = lengths.shape[0]
    value_part = jnp.dot(scaled, value_proj, preferred_element_type=jnp.float32)
    gate_part = jnp.dot(scaled, gate_proj, preferred_element_type=jnp.float32)
    key_part = jnp.dot(scaled, key_proj, preferred_element_type=jnp.float32)
    query_part = jnp.dot(scaled, query_proj, preferred_element_type=jnp.float32)
    step_part = jnp.dot(scaled, step_proj, preferred_element_type=jnp.float32)
    totals = own_rows(lax.psum(squares, "kv"), seq_count)
    value_raw, gate_raw, key_raw, query_raw, step_all = (
        lax.psum_scatter(value_part, "kv", scatter_dimension=0, tiled=True),
        lax.psum_scatter(gate_part, "kv", scatter_dimension=0, tiled=True),
        lax.psum_scatter(key_part, "kv", scatter_dimension=0, tiled=True),
        lax.psum_scatter(query_part, "kv", scatter_dimension=0, tiled=True),
        lax.psum_scatter(step_part, "kv", scatter_dimension=0, tiled=True),
    )
    row_scale = inverse_scale(totals)
    heads_here = decay_rate.shape[0]
    step_raw = (
        lax.dynamic_slice_in_dim(step_all, lax.axis_index("tp") * heads_here, heads_here, 1)
        * row_scale
    )
    new_value = convolve(value_past, value_taps, value_raw * row_scale)
    gate_vals = gate_raw * row_scale
    new_key = convolve(key_past, key_taps, key_raw * row_scale)
    new_query = convolve(query_past, query_taps, query_raw * row_scale)
    step_size = jax.nn.softplus(step_raw)
    new_decay = -decay_rate[None, :] * step_size
    block_len = block_keys.shape[1]
    head_dim = block_state.shape[2]
    state_size = block_state.shape[3]
    per_group = HEADS // GROUPS
    group_count = heads_here // per_group
    live_mask = (jnp.arange(block_len, dtype=jnp.int32)[None, :] < (lengths - 1)[:, None])[
        :, :, None
    ]
    masked = jnp.where(live_mask, block_decay, 0.0)
    running = jnp.cumsum(masked, axis=1)
    block_total = running[:, -1, :]
    tail_sum = block_total[:, None, :] - running
    query_round = new_query.astype(jnp.bfloat16).reshape(seq_count, group_count, state_size)
    scores = jnp.einsum(
        "slgn,sgn->slg",
        block_keys.reshape(seq_count, block_len, group_count, state_size),
        query_round,
        preferred_element_type=jnp.float32,
    )
    scores = jnp.repeat(scores, per_group, axis=2)
    weights = jnp.where(
        live_mask, jnp.exp(tail_sum + new_decay[:, None, :]) * block_steps * scores, 0.0
    ).astype(jnp.bfloat16)
    from_block = jnp.einsum(
        "slh,slhp->shp",
        weights,
        block_values.reshape(seq_count, block_len, heads_here, head_dim),
        preferred_element_type=jnp.float32,
    )
    query_heads = jnp.repeat(
        new_query.reshape(seq_count, group_count, state_size), per_group, axis=1
    )
    source_state = jnp.einsum(
        "shpn,shn->shp", block_state, query_heads, precision=lax.Precision.HIGHEST
    )
    source_state = source_state * jnp.exp(block_total + new_decay)[:, :, None]
    self_score = jnp.repeat(
        jnp.sum((new_query * new_key).reshape(seq_count, group_count, state_size), axis=2),
        per_group,
        axis=1,
    )
    from_token = (step_size * self_score)[:, :, None] * new_value.reshape(
        seq_count, heads_here, head_dim
    )
    gated_out = (source_state + from_block + from_token) * jax.nn.silu(
        gate_vals.reshape(seq_count, heads_here, head_dim)
    )
    normed = gated_out * lax.rsqrt(jnp.mean(gated_out * gated_out, axis=2, keepdims=True) + EPSILON)
    normed = normed * head_gain.reshape(heads_here, head_dim)[None]
    mixed_rows = normed.reshape(seq_count, heads_here * head_dim).astype(jnp.bfloat16)
    partial_value = jnp.dot(
        lax.all_gather(mixed_rows, "kv", axis=0, tiled=True),
        out_proj,
        preferred_element_type=jnp.float32,
    ).astype(jnp.bfloat16)
    return finish(partial_value)


def on_device(
    hidden_in,
    gain_before,
    gate_before,
    lift_before,
    drop_before,
    mixer_gain,
    value_proj,
    gate_proj,
    key_proj,
    query_proj,
    step_proj,
    value_taps,
    key_taps,
    query_taps,
    value_past,
    key_past,
    query_past,
    decay_rate,
    block_state,
    block_keys,
    block_values,
    block_steps,
    block_decay,
    lengths,
    head_gain,
    out_proj,
    gain_after,
    gate_after,
    lift_after,
    drop_after,
):
    section_one = (
        hidden_in.astype(jnp.float32)
        + 0.5 * half_mlp(hidden_in, gain_before, gate_before, lift_before, drop_before)
    ).astype(jnp.bfloat16)
    branch_mix = mixer(
        section_one,
        mixer_gain,
        value_proj,
        gate_proj,
        key_proj,
        query_proj,
        step_proj,
        value_taps,
        key_taps,
        query_taps,
        value_past,
        key_past,
        query_past,
        decay_rate,
        block_state,
        block_keys,
        block_values,
        block_steps,
        block_decay,
        lengths,
        head_gain,
        out_proj,
    )
    section_two = (section_one.astype(jnp.float32) + branch_mix).astype(jnp.bfloat16)
    return (
        section_two.astype(jnp.float32)
        + 0.5 * half_mlp(section_two, gain_after, gate_after, lift_after, drop_after)
    ).astype(jnp.bfloat16)


def solution(mesh):
    return jax.shard_map(
        on_device,
        mesh=mesh,
        in_specs=(
            P("tp", "kv"),
            P("kv"),
            P("kv", "tp"),
            P("kv", "tp"),
            P("tp", "kv"),
            P("kv"),
            P("kv", "tp"),
            P("kv", "tp"),
            P("kv", "tp"),
            P("kv", "tp"),
            P("kv", None),
            P(None, "tp"),
            P(None, "tp"),
            P(None, "tp"),
            P("kv", None, "tp"),
            P("kv", None, "tp"),
            P("kv", None, "tp"),
            P("tp"),
            P("kv", "tp", None, None),
            P("kv", None, "tp"),
            P("kv", None, "tp"),
            P("kv", None, "tp"),
            P("kv", None, "tp"),
            P("kv"),
            P("tp"),
            P("tp", "kv"),
            P("kv"),
            P("kv", "tp"),
            P("kv", "tp"),
            P("tp", "kv"),
        ),
        out_specs=P("tp", "kv"),
        check_vma=False,
    )
```

profile of v0, /device:TPU:0, one launch (start us, length us, event | category | flops | bytes accessed | tf_op | source)
XLA Modules:
  0.0 464.0 jit_solution(2448503861973463744)
XLA Ops:
  6.5 2.3 all_gather.12
  8.8 2.2 fusion.13
  11.1 2.2 fusion.15
  13.5 43.7 %psum.50 = f32[64]{0:T(128)S(1)} all-reduce(f32[64]{0:T(128)S(1)} %fusion.2), channel_id=1, replica_groups=mesh['kv'=16,'tp'=2] {'kv'}, use_global_device_ids=true, to_apply=%region_2.0 | all-reduce | flops 64 | bytes 512 | tf_op jit(solution)/shard_map/psum | solution.py:39
  57.2 75.0 %all-reduce.17.cloned.1.call-done = (f32[64,2816]{1,0:T(8,128)}, f32[64,2816]{1,0:T(8,128)}) async-done(((f32[64,2816]{1,0:T(8,128)}, f32[64,2816]{1,0:T(8,128)}), (f32[64,2816]{1,0:T(8,128)}, f32[64,2816]{1,0:T(8,128)})) %all-reduce.17.cloned.1.call-update) | async-done | bytes 1441808 | tf_op jit(solution)/shard_map/psum | solution.py:42
  132.2 2.6 convolution_convert_fusion.1
  135.0 7.0 %reduce-scatter.4.cloned.1.call-done = bf16[32,128]{1,0:T(8,128)(2,1)} async-done(((bf16[64,128]{1,0:T(8,128)(2,1)}), bf16[32,128]{1,0:T(8,128)(2,1)}) %reduce-scatter.4.cloned.1.call-update) | async-done | bytes 8208 | tf_op jit(solution)/shard_map/reduce_scatter | solution.py:29
  142.7 1.8 all_gather.13
  144.6 0.9 fusion.22
  145.5 0.9 fusion.24
  147.1 0.8 fusion.30
  150.3 2.3 copy.46
  153.0 77.1 %all-reduce.5 = (f32[64]{0:T(128)S(1)}, f32[64,32]{1,0:T(8,128)S(1)}) all-reduce(f32[64]{0:T(128)S(1)} %fusion.4, f32[64,32]{1,0:T(8,128)S(1)} %fusion.28), channel_id=1, replica_groups=mesh['kv'=16,'tp'=2] {'kv'}, use_global_device_ids=true, to_apply=%region_8.9 | all-reduce | flops 2112 | bytes 16896 | tf_op jit(solution)/shard_map/psum | solution.py:87
  230.2 30.9 %all-reduce.15.cloned.1.call-done = (f32[64,1024]{1,0:T(8,128)}, f32[64,1024]{1,0:T(8,128)}, f32[64,512]{1,0:T(8,128)}, f32[64,512]{1,0:T(8,128)}) async-done(((f32[64,1024]{1,0:T(8,128)}, f32[64,1024]{1,0:T(8,128)}, f32[64,512]{1,0:T(8,128)}, f32[64,512]{1,0:T(8,128)}), (f32[64,1024]{1,0:T(8,128)}, f32[64,1024]{1,0:T(8,128)}, f32[64,512]{1,0:T(8,128)}, f32[64,512]{1,0:T(8,128)})) %all-reduce.15.cloned.1.call-update) | async-done | bytes 786448
  261.1 0.8 fusion.17
  263.6 0.9 divide_multiply_fusion
  265.8 1.9 fusion.37
  267.8 3.4 fusion.35
  271.2 0.9 multiply_reduce_fusion.1
  272.7 0.8 reshape.86
  273.5 41.6 %all-gather = bf16[16,4,1024]{2,1,0:T(4,128)(2,1)} all-gather(bf16[1,4,1024]{2,1,0:T(4,128)(2,1)S(1)} %reshape.86), channel_id=1, replica_groups=mesh['kv'=16,'tp'=2] {'kv'}, dimensions={0}, use_global_device_ids=true | all-gather | bytes 139264 | tf_op jit(solution)/shard_map/all_gather | solution.py:158
  315.1 1.6 reshape.87
  316.7 1.8 convolution_convert_fusion.2
  318.6 3.5 reduce-scatter.6.cloned.1.call-done
  323.3 1.8 all_gather.15
  325.1 1.8 fusion.11
  326.9 1.8 fusion.9
  328.9 42.2 %psum.54 = f32[64]{0:T(128)S(1)} all-reduce(f32[64]{0:T(128)S(1)} %fusion.6), channel_id=1, replica_groups=mesh['kv'=16,'tp'=2] {'kv'}, use_global_device_ids=true, to_apply=%region_21.22 | all-reduce | flops 64 | bytes 512 | tf_op jit(solution)/shard_map/psum | solution.py:39
  371.1 75.0 %all-reduce.13.cloned.1.call-done = (f32[64,2816]{1,0:T(8,128)}, f32[64,2816]{1,0:T(8,128)}) async-done(((f32[64,2816]{1,0:T(8,128)}, f32[64,2816]{1,0:T(8,128)}), (f32[64,2816]{1,0:T(8,128)}, f32[64,2816]{1,0:T(8,128)})) %all-reduce.13.cloned.1.call-update) | async-done | bytes 1441808 | tf_op jit(solution)/shard_map/psum | solution.py:42
  446.1 2.6 convolution_convert_fusion
  448.7 7.2 %reduce-scatter.8.cloned.1.call-done = bf16[32,128]{1,0:T(8,128)(2,1)} async-done(((bf16[64,128]{1,0:T(8,128)(2,1)}), bf16[32,128]{1,0:T(8,128)(2,1)}) %reduce-scatter.8.cloned.1.call-update) | async-done | bytes 8208 | tf_op jit(solution)/shard_map/reduce_scatter | solution.py:29
  455.8 1.3 add_convert_fusion
  (114 shorter events, 9.1 us)
Async XLA Ops:
  6.5 261.3 %copy-start = (f32[4,16,64,128]{3,2,1,0:T(8,128)S(1)}, f32[4,16,64,128]{3,2,1,0:T(8,128)}, u32[]{:S(2)}) copy-start(f32[4,16,64,128]{3,2,1,0:T(8,128)} %param.48) | copy-start | bytes 6291460
  6.5 125.6 %all-reduce.17.cloned.1.call-start = ((), (), s32[]{:S(2)}) async-start(), calls=%async_computation.8 | async-start | bytes 2883584 | tf_op jit(solution)/shard_map/psum | solution.py:42
  8.8 48.4 %copy-start.26 = (s32[4]{0:T(128)S(1)}, s32[4]{0:T(128)}, u32[]{:S(2)}) copy-start(s32[4]{0:T(128)} %param.53) | copy-start | bytes 52
  13.3 128.7 %reduce-scatter.4.cloned.1.call-start = ((), (), s32[]{:S(2)}) async-start(), calls=%async_computation.3 | async-start | bytes 24576 | tf_op jit(solution)/shard_map/reduce_scatter | solution.py:29
  132.2 9.9 %copy-start.13 = (bf16[32,128]{1,0:T(8,128)(2,1)S(1)}, bf16[32,128]{1,0:T(8,128)(2,1)}, u32[]{:S(2)}) copy-start(bf16[32,128]{1,0:T(8,128)(2,1)} %param.30) | copy-start | bytes 24580
  132.2 12.4 %copy-start.4 = (bf16[128,1024]{1,0:T(8,128)(2,1)S(1)}, bf16[128,1024]{1,0:T(8,128)(2,1)}, u32[]{:S(2)}) copy-start(bf16[128,1024]{1,0:T(8,128)(2,1)} %param.37) | copy-start | bytes 786436
  132.2 12.4 %copy-start.17 = (f32[128]{0:T(128)S(1)}, f32[128]{0:T(128)}, u32[]{:S(2)}) copy-start(f32[128]{0:T(128)} %param.35) | copy-start | bytes 1540
  132.2 13.3 %copy-start.5 = (bf16[128,1024]{1,0:T(8,128)(2,1)S(1)}, bf16[128,1024]{1,0:T(8,128)(2,1)}, u32[]{:S(2)}) copy-start(bf16[128,1024]{1,0:T(8,128)(2,1)} %param.36) | copy-start | bytes 786436
  132.2 14.2 %copy-start.6 = (bf16[128,512]{1,0:T(8,128)(2,1)S(1)}, bf16[128,512]{1,0:T(8,128)(2,1)}, u32[]{:S(2)}) copy-start(bf16[128,512]{1,0:T(8,128)(2,1)} %param.38) | copy-start | bytes 393220
  132.2 14.9 %copy-start.7 = (bf16[128,512]{1,0:T(8,128)(2,1)S(1)}, bf16[128,512]{1,0:T(8,128)(2,1)}, u32[]{:S(2)}) copy-start(bf16[128,512]{1,0:T(8,128)(2,1)} %param.39) | copy-start | bytes 393220
  134.8 13.2 %copy-start.14 = (f32[4,128,16]{1,2,0:T(8,128)S(1)}, f32[4,128,16]{1,2,0:T(8,128)}, u32[]{:S(2)}) copy-start(f32[4,128,16]{1,2,0:T(8,128)} %param.52) | copy-start | bytes 98308
  134.8 13.2 %copy-start.19 = (f32[4,512]{1,0:T(4,128)S(1)}, f32[4,512]{1,0:T(4,128)}, u32[]{:S(2)}) copy-start(f32[4,512]{1,0:T(4,128)} %param.43) | copy-start | bytes 24580
  134.8 13.2 %copy-start.18 = (f32[4,512]{1,0:T(4,128)S(1)}, f32[4,512]{1,0:T(4,128)}, u32[]{:S(2)}) copy-start(f32[4,512]{1,0:T(4,128)} %param.42) | copy-start | bytes 24580
  134.8 13.3 %copy-start.3 = (bf16[4,128,512]{2,1,0:T(8,128)(2,1)S(1)}, bf16[4,128,512]{2,1,0:T(8,128)(2,1)}, u32[]{:S(2)}) copy-start(bf16[4,128,512]{2,1,0:T(8,128)(2,1)} %param.49) | copy-start | bytes 1572868
  134.9 126.2 %all-reduce.15.cloned.1.call-start = ((), (), s32[]{:S(2)}) async-start(), calls=%async_computation.7 | async-start | bytes 1572864
  135.0 13.1 %copy-start.24 = (pred[4,128]{1,0:T(4,128)(4,1)}, pred[4,128]{1,0:T(4,128)(4,1)S(1)}, u32[]{:S(2)}) copy-start(pred[4,128]{1,0:T(4,128)(4,1)S(1)} %iota_compare_fusion) | copy-start | bytes 1540
  144.6 5.6 %copy-start.27 = (f32[16]{0:T(128)S(1)}, f32[16]{0:T(128)}, u32[]{:S(2)}) copy-start(f32[16]{0:T(128)} %param.47) | copy-start | bytes 196
  144.6 5.6 %copy-start.12 = (f32[4,128,16]{1,2,0:T(8,128)S(1)}, f32[4,128,16]{1,2,0:T(8,128)}, u32[]{:S(2)}) copy-start(f32[4,128,16]{1,2,0:T(8,128)} %param.51) | copy-start | bytes 98308
  148.0 174.1 %reduce-scatter.6.cloned.1.call-start = ((), (), s32[]{:S(2)}) async-start(), calls=%async_computation.4 | async-start | bytes 24576 | tf_op jit(solution)/shard_map/reduce_scatter | solution.py:29
  148.1 4.4 copy-start.15
  148.1 4.5 copy-start.16
  148.1 4.5 copy-start.20
  148.2 4.5 copy-start.21
  148.2 4.7 %copy-start.22 = (bf16[128,32]{0,1:T(8,128)(2,1)S(1)}, bf16[128,32]{0,1:T(8,128)(2,1)}, u32[]{:S(2)}) copy-start(bf16[128,32]{0,1:T(8,128)(2,1)} %param.40) | copy-start | bytes 24580
  148.6 114.7 %copy-start.25 = (pred[4,128]{1,0:T(4,128)(4,1)S(1)}, pred[4,128]{1,0:T(4,128)(4,1)}, u32[]{:S(2)}) copy-start(pred[4,128]{1,0:T(4,128)(4,1)} %copy-done.24) | copy-start | bytes 1540
  265.8 5.3 %copy-start.8 = (f32[4,16,64]{2,1,0:T(8,128)S(1)}, f32[4,16,64]{2,1,0:T(8,128)}, u32[]{:S(2)}) copy-start(f32[4,16,64]{2,1,0:T(8,128)} %reshape.84) | copy-start | bytes 49156
  265.8 5.3 %copy-start.9 = (f32[4,16,64]{2,1,0:T(8,128)S(1)}, f32[4,16,64]{2,1,0:T(8,128)}, u32[]{:S(2)}) copy-start(f32[4,16,64]{2,1,0:T(8,128)} %reshape.85) | copy-start | bytes 49156
  265.8 59.3 %copy-start.1 = (bf16[128,2816]{1,0:T(8,128)(2,1)S(1)}, bf16[128,2816]{1,0:T(8,128)(2,1)}, u32[]{:S(2)}) copy-start(bf16[128,2816]{1,0:T(8,128)(2,1)} %param.57) | copy-start | bytes 2162692
  267.8 59.1 %copy-start.2 = (bf16[128,2816]{1,0:T(8,128)(2,1)S(1)}, bf16[128,2816]{1,0:T(8,128)(2,1)}, u32[]{:S(2)}) copy-start(bf16[128,2816]{1,0:T(8,128)(2,1)} %param.58) | copy-start | bytes 2162692
  318.5 127.6 %all-reduce.13.cloned.1.call-start = ((), (), s32[]{:S(2)}) async-start(), calls=%async_computation.6 | async-start | bytes 2883584 | tf_op jit(solution)/shard_map/psum | solution.py:42
  328.7 127.1 %reduce-scatter.8.cloned.1.call-start = ((), (), s32[]{:S(2)}) async-start(), calls=%async_computation.5 | async-start | bytes 24576 | tf_op jit(solution)/shard_map/reduce_scatter | solution.py:29
  446.1 9.8 %copy-start.11 = (bf16[32,128]{1,0:T(8,128)(2,1)S(1)}, bf16[32,128]{1,0:T(8,128)(2,1)}, u32[]{:S(2)}) copy-start(bf16[32,128]{1,0:T(8,128)(2,1)} %copy-done.10) | copy-start | bytes 24580
  (3 other events, 9.4 us)
Sparse Core Ops, SparseCore 0:
  13.5 118.6 all-reduce.16
  135.0 6.9 reduce-scatter.3
  148.1 112.9 all-reduce.14
  318.6 3.3 reduce-scatter.5
  328.8 117.2 all-reduce.12
  448.8 6.9 reduce-scatter.7
where the time goes:
time: 465 us; the launch traced here: 464 us
  blocking collectives  211 us (45%)
  waiting for transfers between devices  199 us (43%)
  matrix products  24 us (5%)
  between operations  14.5 us (3%)
  local copies, waits for them, and re-layouts  8.42 us (2%)
  other arithmetic  7.7 us (2%)
    psum x2, waiting for transfers between devices, half_mlp(): gate_sum, lift_sum = lax.psum((gate_part, lift_part), 'kv')  150 us
    psum x2, blocking collectives, half_mlp(): totals = lax.psum(squares, 'kv')  85.9 us
    psum x1, blocking collectives, mixer(): totals = own_rows(lax.psum(squares, 'kv'), seq_count)  77.1 us
    all_gather x1, blocking collectives, mixer(): lax.all_gather(mixed_rows, 'kv', axis=0, tiled=True)  41.6 us
    unnamed x7, waiting for transfers between devices  31 us
    reduce_scatter x3, waiting for transfers between devices, finish(): lax.psum_scatter(partial_value.astype(jnp.float32).astype(jnp.bfloat16),...  17.7 us
  transfers between devices with their start and end apart: 6, of which 6 were waited for; matrix products, arithmetic and copies ran while one was open for 1% of the time, Pallas kernels for 0%

commit v1 on v0

--- a/solution.py
+++ b/solution.py
@@ -36,7 +36,9 @@
 
 def half_mlp(rows_in, gain_vec, gate_weight, lift_weight, drop_weight):
     scaled, squares = gather_rows(rows_in, gain_vec)
-    totals = lax.psum(squares, "kv")
+    totals = squares
+    for hop in (1, 2, 4, 8):
+        totals = totals + lax.ppermute(totals, "kv", [(dev, dev ^ hop) for dev in range(16)])
     gate_part = jnp.dot(scaled, gate_weight, preferred_element_type=jnp.float32)
     lift_part = jnp.dot(scaled, lift_weight, preferred_element_type=jnp.float32)
     gate_sum, lift_sum = lax.psum((gate_part, lift_part), "kv")

time: 465 us -> 465 us (level)
  blocking collectives: 211 us -> 125 us
  waiting for transfers between devices: 199 us -> 267 us
  starting transfers between devices: 0.21 us -> 17.6 us
    psum x2 -> x0, blocking collectives: 85.9 us -> none  [half_mlp(): totals = lax.psum(squares, 'kv')]
    psum x2, waiting for transfers between devices: 150 us -> 204 us  [half_mlp(): gate_sum, lift_sum = lax.psum((gate_part, lift_part), 'kv')]
    ppermute x0 -> x8, starting transfers between devices: none -> 17.4 us  [half_mlp(): lax.ppermute(totals, 'kv', [(dev, dev ^ hop) for dev in range(16)])]
    ppermute x0 -> x8, waiting for transfers between devices: none -> 14.7 us  [half_mlp(): lax.ppermute(totals, 'kv', [(dev, dev ^ hop) for dev in range(16)])]
  transfers between devices with their start and end apart: 6 -> 14, of which waited for: 6 -> 14; matrix products, arithmetic and copies ran while one was open for 1% -> 1% of each run, Pallas kernels for 0% -> 0%
where the time goes in v1:
time: 465 us; the launch traced here: 464 us
  waiting for transfers between devices  267 us (57%)
  blocking collectives  125 us (27%)
  matrix products  24 us (5%)
  starting transfers between devices  17.6 us (4%)
  between operations  14.5 us (3%)
  local copies, waits for them, and re-layouts  8.43 us (2%)
  other arithmetic  7.72 us (2%)
    psum x2, waiting for transfers between devices, half_mlp(): gate_sum, lift_sum = lax.psum((gate_part, lift_part), 'kv')  204 us
    psum x1, blocking collectives, mixer(): totals = own_rows(lax.psum(squares, 'kv'), seq_count)  77.2 us
    all_gather x1, blocking collectives, mixer(): lax.all_gather(mixed_rows, 'kv', axis=0, tiled=True)  41.6 us
    unnamed x7, waiting for transfers between devices  31 us
    reduce_scatter x3, waiting for transfers between devices, finish(): lax.psum_scatter(partial_value.astype(jnp.float32).astype(jnp.bfloat16),...  17.7 us
    ppermute x8, starting transfers between devices, half_mlp(): lax.ppermute(totals, 'kv', [(dev, dev ^ hop) for dev in range(16)])  17.4 us
    ppermute x8, waiting for transfers between devices, half_mlp(): lax.ppermute(totals, 'kv', [(dev, dev ^ hop) for dev in range(16)])  14.7 us
  transfers between devices with their start and end apart: 14, of which 14 were waited for; matrix products, arithmetic and copies ran while one was open for 1% of the time, Pallas kernels for 0%

profile of v1, /device:TPU:0, one launch (start us, length us, event | category | flops | bytes accessed | tf_op | source)
XLA Modules:
  0.0 464.1 jit_solution(13339581685637497307)
XLA Ops:
  6.5 2.3 all_gather.12
  8.8 2.3 fusion.13
  11.1 2.2 fusion.15
  13.5 2.9 collective-permute-start
  18.0 2.0 collective-permute-start.1
  21.6 2.1 collective-permute-start.2
  23.6 2.0 collective-permute-done.2
  25.6 2.7 collective-permute-start.3
  28.4 1.8 collective-permute-done.3
  30.1 102.0 %all-reduce.17.cloned.1.call-done = (f32[64,2816]{1,0:T(8,128)}, f32[64,2816]{1,0:T(8,128)}) async-done(((f32[64,2816]{1,0:T(8,128)}, f32[64,2816]{1,0:T(8,128)}), (f32[64,2816]{1,0:T(8,128)}, f32[64,2816]{1,0:T(8,128)})) %all-reduce.17.cloned.1.call-update) | async-done | bytes 1441808 | tf_op jit(solution)/shard_map/psum | solution.py:44
  132.2 2.6 convolution_convert_fusion.1
  135.0 7.0 %reduce-scatter.4.cloned.1.call-done = bf16[32,128]{1,0:T(8,128)(2,1)} async-done(((bf16[64,128]{1,0:T(8,128)(2,1)}), bf16[32,128]{1,0:T(8,128)(2,1)}) %reduce-scatter.4.cloned.1.call-update) | async-done | bytes 8208 | tf_op jit(solution)/shard_map/reduce_scatter | solution.py:29
  142.7 1.8 all_gather.13
  150.3 2.3 copy.46
  153.0 77.2 %all-reduce.5 = (f32[64]{0:T(128)S(1)}, f32[64,32]{1,0:T(8,128)S(1)}) all-reduce(f32[64]{0:T(128)S(1)} %fusion.4, f32[64,32]{1,0:T(8,128)S(1)} %fusion.28), channel_id=1, replica_groups=mesh['kv'=16,'tp'=2] {'kv'}, use_global_device_ids=true, to_apply=%region_7.8 | all-reduce | flops 2112 | bytes 16896 | tf_op jit(solution)/shard_map/psum | solution.py:89
  230.2 30.9 %all-reduce.15.cloned.1.call-done = (f32[64,1024]{1,0:T(8,128)}, f32[64,1024]{1,0:T(8,128)}, f32[64,512]{1,0:T(8,128)}, f32[64,512]{1,0:T(8,128)}) async-done(((f32[64,1024]{1,0:T(8,128)}, f32[64,1024]{1,0:T(8,128)}, f32[64,512]{1,0:T(8,128)}, f32[64,512]{1,0:T(8,128)}), (f32[64,1024]{1,0:T(8,128)}, f32[64,1024]{1,0:T(8,128)}, f32[64,512]{1,0:T(8,128)}, f32[64,512]{1,0:T(8,128)})) %all-reduce.15.cloned.1.call-update) | async-done | bytes 786448
  265.9 1.9 fusion.37
  267.9 3.4 fusion.35
  273.6 41.6 %all-gather = bf16[16,4,1024]{2,1,0:T(4,128)(2,1)} all-gather(bf16[1,4,1024]{2,1,0:T(4,128)(2,1)S(1)} %reshape.86), channel_id=1, replica_groups=mesh['kv'=16,'tp'=2] {'kv'}, dimensions={0}, use_global_device_ids=true | all-gather | bytes 139264 | tf_op jit(solution)/shard_map/all_gather | solution.py:160
  316.7 1.8 convolution_convert_fusion.2
  318.6 3.5 reduce-scatter.6.cloned.1.call-done
  323.4 1.8 all_gather.15
  325.2 1.8 fusion.11
  327.0 1.8 fusion.9
  330.7 1.9 collective-permute-done.4
  334.3 1.9 collective-permute-done.5
  337.8 2.1 collective-permute-done.6
  340.0 2.5 collective-permute-start.7
  342.5 2.0 collective-permute-done.7
  344.5 101.7 %all-reduce.13.cloned.1.call-done = (f32[64,2816]{1,0:T(8,128)}, f32[64,2816]{1,0:T(8,128)}) async-done(((f32[64,2816]{1,0:T(8,128)}, f32[64,2816]{1,0:T(8,128)}), (f32[64,2816]{1,0:T(8,128)}, f32[64,2816]{1,0:T(8,128)})) %all-reduce.13.cloned.1.call-update) | async-done | bytes 1441808 | tf_op jit(solution)/shard_map/psum | solution.py:44
  446.2 2.6 convolution_convert_fusion
  448.7 7.2 %reduce-scatter.8.cloned.1.call-done = bf16[32,128]{1,0:T(8,128)(2,1)} async-done(((bf16[64,128]{1,0:T(8,128)(2,1)}), bf16[32,128]{1,0:T(8,128)(2,1)}) %reduce-scatter.8.cloned.1.call-update) | async-done | bytes 8208 | tf_op jit(solution)/shard_map/reduce_scatter | solution.py:29
  (134 shorter events, 26.2 us)
Async XLA Ops:
  6.5 261.3 %copy-start = (f32[4,16,64,128]{3,2,1,0:T(8,128)S(1)}, f32[4,16,64,128]{3,2,1,0:T(8,128)}, u32[]{:S(2)}) copy-start(f32[4,16,64,128]{3,2,1,0:T(8,128)} %param.48) | copy-start | bytes 6291460
  6.5 125.6 %all-reduce.17.cloned.1.call-start = ((), (), s32[]{:S(2)}) async-start(), calls=%async_computation.8 | async-start | bytes 2883584 | tf_op jit(solution)/shard_map/psum | solution.py:44
  8.8 19.5 %copy-start.26 = (s32[4]{0:T(128)S(1)}, s32[4]{0:T(128)}, u32[]{:S(2)}) copy-start(s32[4]{0:T(128)} %param.53) | copy-start | bytes 52
  13.4 128.6 %reduce-scatter.4.cloned.1.call-start = ((), (), s32[]{:S(2)}) async-start(), calls=%async_computation.3 | async-start | bytes 24576 | tf_op jit(solution)/shard_map/reduce_scatter | solution.py:29
  13.5 4.4 collective-permute-start
  18.0 3.6 collective-permute-start.1
  21.6 4.1 collective-permute-start.2
  25.6 4.5 collective-permute-start.3
  132.1 9.8 %copy-start.13 = (bf16[32,128]{1,0:T(8,128)(2,1)S(1)}, bf16[32,128]{1,0:T(8,128)(2,1)}, u32[]{:S(2)}) copy-start(bf16[32,128]{1,0:T(8,128)(2,1)} %param.30) | copy-start | bytes 24580
  132.2 12.4 %copy-start.4 = (bf16[128,1024]{1,0:T(8,128)(2,1)S(1)}, bf16[128,1024]{1,0:T(8,128)(2,1)}, u32[]{:S(2)}) copy-start(bf16[128,1024]{1,0:T(8,128)(2,1)} %param.37) | copy-start | bytes 786436
  132.2 12.4 %copy-start.17 = (f32[128]{0:T(128)S(1)}, f32[128]{0:T(128)}, u32[]{:S(2)}) copy-start(f32[128]{0:T(128)} %param.35) | copy-start | bytes 1540
  132.2 13.3 %copy-start.5 = (bf16[128,1024]{1,0:T(8,128)(2,1)S(1)}, bf16[128,1024]{1,0:T(8,128)(2,1)}, u32[]{:S(2)}) copy-start(bf16[128,1024]{1,0:T(8,128)(2,1)} %param.36) | copy-start | bytes 786436
  132.2 14.2 %copy-start.6 = (bf16[128,512]{1,0:T(8,128)(2,1)S(1)}, bf16[128,512]{1,0:T(8,128)(2,1)}, u32[]{:S(2)}) copy-start(bf16[128,512]{1,0:T(8,128)(2,1)} %param.38) | copy-start | bytes 393220
  132.2 15.0 %copy-start.7 = (bf16[128,512]{1,0:T(8,128)(2,1)S(1)}, bf16[128,512]{1,0:T(8,128)(2,1)}, u32[]{:S(2)}) copy-start(bf16[128,512]{1,0:T(8,128)(2,1)} %param.39) | copy-start | bytes 393220
  134.8 13.2 %copy-start.14 = (f32[4,128,16]{1,2,0:T(8,128)S(1)}, f32[4,128,16]{1,2,0:T(8,128)}, u32[]{:S(2)}) copy-start(f32[4,128,16]{1,2,0:T(8,128)} %param.52) | copy-start | bytes 98308
  134.8 13.3 %copy-start.19 = (f32[4,512]{1,0:T(4,128)S(1)}, f32[4,512]{1,0:T(4,128)}, u32[]{:S(2)}) copy-start(f32[4,512]{1,0:T(4,128)} %param.43) | copy-start | bytes 24580
  134.8 13.3 %copy-start.18 = (f32[4,512]{1,0:T(4,128)S(1)}, f32[4,512]{1,0:T(4,128)}, u32[]{:S(2)}) copy-start(f32[4,512]{1,0:T(4,128)} %param.42) | copy-start | bytes 24580
  134.8 13.3 %copy-start.3 = (bf16[4,128,512]{2,1,0:T(8,128)(2,1)S(1)}, bf16[4,128,512]{2,1,0:T(8,128)(2,1)}, u32[]{:S(2)}) copy-start(bf16[4,128,512]{2,1,0:T(8,128)(2,1)} %param.49) | copy-start | bytes 1572868
  134.8 126.3 %all-reduce.15.cloned.1.call-start = ((), (), s32[]{:S(2)}) async-start(), calls=%async_computation.7 | async-start | bytes 1572864
  135.0 13.1 %copy-start.24 = (pred[4,128]{1,0:T(4,128)(4,1)}, pred[4,128]{1,0:T(4,128)(4,1)S(1)}, u32[]{:S(2)}) copy-start(pred[4,128]{1,0:T(4,128)(4,1)S(1)} %iota_compare_fusion) | copy-start | bytes 1540
  144.5 5.6 %copy-start.12 = (f32[4,128,16]{1,2,0:T(8,128)S(1)}, f32[4,128,16]{1,2,0:T(8,128)}, u32[]{:S(2)}) copy-start(f32[4,128,16]{1,2,0:T(8,128)} %param.51) | copy-start | bytes 98308
  148.0 174.1 %reduce-scatter.6.cloned.1.call-start = ((), (), s32[]{:S(2)}) async-start(), calls=%async_computation.4 | async-start | bytes 24576 | tf_op jit(solution)/shard_map/reduce_scatter | solution.py:29
  148.6 114.8 %copy-start.25 = (pred[4,128]{1,0:T(4,128)(4,1)S(1)}, pred[4,128]{1,0:T(4,128)(4,1)}, u32[]{:S(2)}) copy-start(pred[4,128]{1,0:T(4,128)(4,1)} %copy-done.24) | copy-start | bytes 1540
  265.9 59.3 %copy-start.1 = (bf16[128,2816]{1,0:T(8,128)(2,1)S(1)}, bf16[128,2816]{1,0:T(8,128)(2,1)}, u32[]{:S(2)}) copy-start(bf16[128,2816]{1,0:T(8,128)(2,1)} %param.57) | copy-start | bytes 2162692
  267.8 59.1 %copy-start.2 = (bf16[128,2816]{1,0:T(8,128)(2,1)S(1)}, bf16[128,2816]{1,0:T(8,128)(2,1)}, u32[]{:S(2)}) copy-start(bf16[128,2816]{1,0:T(8,128)(2,1)} %param.58) | copy-start | bytes 2162692
  318.6 127.6 %all-reduce.13.cloned.1.call-start = ((), (), s32[]{:S(2)}) async-start(), calls=%async_computation.6 | async-start | bytes 2883584 | tf_op jit(solution)/shard_map/psum | solution.py:44
  328.8 127.1 %reduce-scatter.8.cloned.1.call-start = ((), (), s32[]{:S(2)}) async-start(), calls=%async_computation.5 | async-start | bytes 24576 | tf_op jit(solution)/shard_map/reduce_scatter | solution.py:29
  328.9 3.6 collective-permute-start.4
  332.6 3.6 collective-permute-start.5
  336.1 3.8 collective-permute-start.6
  340.0 4.5 collective-permute-start.7
  446.2 9.7 %copy-start.11 = (bf16[32,128]{1,0:T(8,128)(2,1)S(1)}, bf16[32,128]{1,0:T(8,128)(2,1)}, u32[]{:S(2)}) copy-start(bf16[32,128]{1,0:T(8,128)(2,1)} %copy-done.10) | copy-start | bytes 24580
  (11 other events, 48.4 us)
Sparse Core Ops, SparseCore 0:
  13.5 118.6 all-reduce.16
  135.0 6.9 reduce-scatter.3
  148.1 113.0 all-reduce.14
  318.7 3.3 reduce-scatter.5
  328.9 117.2 all-reduce.12
  448.9 6.9 reduce-scatter.7
